TPU v7x, 32 devices: a whole 2x2x4 slice. The times are simulated.
32 devices in a mesh: sp: 4 (over z), fs: 4 (over y, x), tp: 2 (over core).
Axes of the slice: x: 2, y: 2, z: 4, core: 2. Of those that a mesh axis runs over, the one named last changes fastest.
Arguments:
- tokens: bfloat16 [1024, 2048], P('sp'), may hold values from -6 to 6
- norm_gain: float32 [2048], replicated, may hold values from 0.1 to 1.9
- conv_value: bfloat16 [2048, 1024], P('sp', ('fs', 'tp')), may hold values from -0.125 to 0.125
- conv_gate: bfloat16 [2048, 1024], P('sp', ('fs', 'tp')), may hold values from -0.125 to 0.125
- mixer_gate: bfloat16 [2048, 1024], P('sp', ('fs', 'tp')), may hold values from -0.125 to 0.125
- state_input: bfloat16 [2048, 1024], P('sp', ('fs', 'tp')), may hold values from -0.125 to 0.125
- write_projection: bfloat16 [2048, 1024], P('sp', ('fs', 'tp')), may hold values from -0.125 to 0.125
- state_read: bfloat16 [2048, 1024], P('sp', ('fs', 'tp')), may hold values from -0.125 to 0.125
- step_proj: bfloat16 [2048, 16], replicated, may hold values from -0.125 to 0.125
- step_bias: float32 [16], P(('fs', 'tp')), may hold values from -6 to -0.5
- decay_log: float32 [16], P(('fs', 'tp')), may hold values from -9 to -1.5
- decay_extra: float32 [16, 1024], P(('fs', 'tp'), 'sp'), may hold values from -0.8 to 0
- input_taps: float32 [4, 1024], P(None, ('fs', 'tp')), may hold values from -3 to 3
- write_taps: float32 [4, 1024], P(None, ('fs', 'tp')), may hold values from -3 to 3
- fetch_kernel_coefficients: float32 [4, 1024], P(None, ('fs', 'tp')), may hold values from -3 to 3
- long_taps: float32 [31, 1024], P(None, ('fs', 'tp')), may hold values from -5 to 5
- conv_gain: float32 [1024], P(('fs', 'tp')), may hold values from 0.1 to 1.9
- state_gain: float32 [1024], P(('fs', 'tp')), may hold values from 0.1 to 1.9
- conv_output: bfloat16 [2048, 1024], P('sp', ('fs', 'tp')), may hold values from -0.125 to 0.125
- state_output: bfloat16 [2048, 1024], P('sp', ('fs', 'tp')), may hold values from -0.125 to 0.125
- initial_state: float32 [16, 64, 128], P(('fs', 'tp')), may hold values from -12 to 12
Outputs:
- mixed: bfloat16 [1024, 2048], P(('sp', 'fs', 'tp'))
All inputs are finite; a program needn't handle non-finite values.
Results may differ from a plain program's by a relative error of at most 0.017.
Values may be sent and summed in bfloat16 or wider, within the bound.
A program may use at most 64 MiB of HBM per device.

v0:
```python
import jax
import jax.numpy as jnp
from jax import lax
from jax.sharding import PartitionSpec as P

C_CH = 1024
STATE = 128
WIDE_TAPS = 31
SHORT_TAPS = 4
SPAN = 64
D_INNER = 1024


eps_norm = 1e-06


def shifted(block, axis, distance):
    devices = range(lax.axis_size(axis))
    route = [(i - distance, i) for i in devices if i - distance in devices]
    return lax.ppermute(block, axis, route)


def causal_valid(padded, taps):
    result = lax.conv_general_dilated(
        padded[None],
        taps[:, None, :],
        window_strides=(1,),
        padding="VALID",
        dimension_numbers=("NWC", "WIO", "NWC"),
        feature_group_count=taps.shape[1],
        precision=lax.Precision.HIGHEST,
    )
    return result[0]


def project(normed, weight):
    return jnp.dot(normed, weight, preferred_element_type=jnp.float32).astype(jnp.bfloat16)


def carry_step(state, inputs):
    fresh, last = inputs
    return (state * jnp.exp(last)[:, None, None] + fresh, state)


def per_device(
    tokens,
    norm_gain,
    conv_value,
    conv_gate,
    mixer_gate,
    state_input,
    write_projection,
    state_read,
    step_proj,
    step_bias,
    decay_log,
    decay_extra,
    input_taps,
    write_taps,
    fetch_kernel_coefficients,
    long_taps,
    conv_gain,
    state_gain,
    conv_output,
    state_output,
    initial_state,
):
    rows = tokens.shape[0]
    channels = conv_value.shape[1]
    width_in = state_input.shape[1]
    width_group = write_projection.shape[1]
    heads = step_bias.shape[0]
    groups = width_group // STATE
    per_group = heads // groups
    head_size = width_in // heads
    values = tokens.astype(jnp.float32)
    normed = (
        values * lax.rsqrt(jnp.mean(values * values, axis=1, keepdims=True) + eps_norm) * norm_gain
    ).astype(jnp.bfloat16)
    (
        whole_value,
        whole_gate,
        whole_input,
        whole_write,
        whole_read,
        whole_mixer,
        back_conv,
        back_state,
    ) = (
        lax.all_gather(conv_value, "sp", axis=0, tiled=True),
        lax.all_gather(conv_gate, "sp", axis=0, tiled=True),
        lax.all_gather(state_input, "sp", axis=0, tiled=True),
        lax.all_gather(write_projection, "sp", axis=0, tiled=True),
        lax.all_gather(state_read, "sp", axis=0, tiled=True),
        lax.all_gather(mixer_gate, "sp", axis=0, tiled=True),
        lax.all_gather(conv_output, "sp", axis=0, tiled=True),
        lax.all_gather(state_output, "sp", axis=0, tiled=True),
    )
    input_rows = project(normed, whole_input)
    write_rows = project(normed, whole_write)
    read_rows = project(normed, whole_read)
    gate_z = project(normed, whole_mixer)
    value_rows = project(normed, whole_value)
    gate_rows = project(normed, whole_gate)
    step_all = jnp.dot(normed, step_proj, preferred_element_type=jnp.float32)
    head_start = (lax.axis_index("fs") * lax.axis_size("tp") + lax.axis_index("tp")) * heads
    step_raw = lax.dynamic_slice_in_dim(step_all, head_start, heads, 1)
    step_size = jax.nn.softplus(step_raw + step_bias)
    log_step = -jnp.exp(decay_log) * step_size + decay_extra.T
    edge_width = WIDE_TAPS - 1
    tail = rows - edge_width
    packed = jnp.concatenate(
        [
            value_rows[tail:],
            gate_rows[tail:],
            input_rows[tail:],
            write_rows[tail:],
            read_rows[tail:],
        ],
        axis=1,
    )
    before = shifted(packed, "sp", 1)
    short_edge = before[edge_width - SHORT_TAPS + 1 :, 2 * channels :]
    state_row_values = jnp.concatenate([input_rows, write_rows, read_rows], axis=1)
    state_full = jnp.concatenate([short_edge, state_row_values], axis=0).astype(jnp.float32)
    state_taps = jnp.concatenate([input_taps, write_taps, fetch_kernel_coefficients], axis=1)
    activated = jax.nn.silu(causal_valid(state_full, state_taps))
    input_act = activated[:, :width_in]
    write_activation = activated[:, width_in : width_in + width_group]
    read_act = activated[:, width_in + width_group :]
    blocks = rows // SPAN
    x_heads = (input_act.reshape(rows, heads, head_size) * step_size[:, :, None]).reshape(
        blocks, SPAN, heads, head_size
    )
    write_heads = jnp.repeat(
        write_activation.reshape(rows, groups, STATE), per_group, axis=1
    ).reshape(blocks, SPAN, heads, STATE)
    read_heads = jnp.repeat(read_act.reshape(rows, groups, STATE), per_group, axis=1).reshape(
        blocks, SPAN, heads, STATE
    )
    log_blocks = log_step.reshape(blocks, SPAN, heads)
    cumul = jnp.cumsum(log_blocks, axis=1)
    lower = jnp.tril(jnp.ones((SPAN, SPAN), dtype=bool))
    by_head = jnp.swapaxes(cumul, 1, 2)
    gaps = by_head[:, :, :, None] - by_head[:, :, None, :]
    weights = jnp.where(lower, jnp.exp(jnp.where(lower, gaps, 0.0)), 0.0)
    scores = jnp.einsum("bthn,bshn->bhts", read_heads, write_heads, precision=lax.Precision.HIGHEST)
    inner = jnp.einsum(
        "bhts,bshp->bthp", scores * weights, x_heads, precision=lax.Precision.HIGHEST
    )
    last = cumul[:, -1]
    fresh = jnp.einsum(
        "bshn,bshp->bhpn",
        write_heads * jnp.exp(last[:, None, :] - cumul)[:, :, :, None],
        x_heads,
        precision=lax.Precision.HIGHEST,
    )
    state_end, block_states = lax.scan(
        carry_step, jnp.zeros((heads, head_size, STATE), jnp.float32), (fresh, last)
    )
    logsum = jnp.sum(last, axis=0)
    block_prefix = jnp.cumsum(last, axis=0) - last
    start_decay = jnp.exp(block_prefix[:, None, :] + cumul)
    local_out = (
        inner
        + jnp.einsum("bthn,bhpn->bthp", read_heads, block_states, precision=lax.Precision.HIGHEST)
        * jnp.exp(cumul)[:, :, :, None]
    )
    value_full = jnp.concatenate([before[:, :channels], value_rows], axis=0).astype(jnp.float32)
    gate_full = jnp.concatenate([before[:, channels : 2 * channels], gate_rows], axis=0).astype(
        jnp.float32
    )
    glu = value_full * jax.nn.sigmoid(gate_full)
    long_mix = causal_valid(glu, long_taps)
    total_sum, total_square = lax.psum(
        (jnp.sum(long_mix, axis=1), jnp.sum(long_mix * long_mix, axis=1)), ("fs", "tp")
    )
    mean = total_sum / C_CH
    spread = total_square / C_CH - mean * mean
    conv_out = jax.nn.silu(
        (long_mix - mean[:, None]) * lax.rsqrt(spread + eps_norm)[:, None] * conv_gain
    ).astype(jnp.bfloat16)
    totals = lax.all_gather(logsum[None], "sp", axis=0, tiled=True)
    inclusive = jnp.cumsum(totals, axis=0)
    position = lax.axis_index("sp")
    prefix_log = lax.dynamic_index_in_dim(inclusive - totals, position, 0, keepdims=False)
    piece = lax.all_gather(state_end[None].astype(jnp.bfloat16), "sp", axis=0, tiled=True).astype(
        jnp.float32
    )
    count = piece.shape[0]
    order = jnp.arange(count, dtype=jnp.int32)
    live = (order < position)[:, None]
    factor = jnp.where(live, jnp.exp(jnp.where(live, prefix_log[None, :] - inclusive, 0.0)), 0.0)
    entering = jnp.zeros_like(state_end) + jnp.einsum(
        "kh,khpn->hpn", factor, piece, precision=lax.Precision.HIGHEST
    )
    start_state = entering + jnp.exp(prefix_log)[:, None, None] * initial_state
    outputs = (
        local_out
        + jnp.einsum("bthn,hpn->bthp", read_heads, start_state, precision=lax.Precision.HIGHEST)
        * start_decay[:, :, :, None]
    )
    gated = outputs.reshape(rows, width_in) * jax.nn.silu(gate_z.astype(jnp.float32))
    quadratic_total = lax.psum(jnp.sum(gated * gated, axis=1), ("fs", "tp"))
    state_out = (
        gated * lax.rsqrt(quadratic_total / D_INNER + eps_norm)[:, None] * state_gain
    ).astype(jnp.bfloat16)
    contract = (((1,), (1,)), ((), ()))
    out_rows = rows // (lax.axis_size("fs") * lax.axis_size("tp"))
    conv_part = lax.slice_in_dim(conv_out, 0, out_rows * lax.axis_size(("fs", "tp")), axis=0)
    term = lax.dot_general(conv_part, back_conv, contract, preferred_element_type=jnp.float32)
    return lax.psum_scatter(
        (
            term
            + lax.dot_general(state_out, back_state, contract, preferred_element_type=jnp.float32)
        ).astype(jnp.bfloat16),
        ("fs", "tp"),
        scatter_dimension=0,
        tiled=True,
    )


def solution(mesh):
    placed = (
        P("sp", None),
        P(),
        P("sp", ("fs", "tp")),
        P("sp", ("fs", "tp")),
        P("sp", ("fs", "tp")),
        P("sp", ("fs", "tp")),
        P("sp", ("fs", "tp")),
        P("sp", ("fs", "tp")),
        P(),
        P(("fs", "tp")),
        P(("fs", "tp")),
        P(("fs", "tp"), "sp"),
        P(None, ("fs", "tp")),
        P(None, ("fs", "tp")),
        P(None, ("fs", "tp")),
        P(None, ("fs", "tp")),
        P(("fs", "tp")),
        P(("fs", "tp")),
        P("sp", ("fs", "tp")),
        P("sp", ("fs", "tp")),
        P(("fs", "tp"), None, None),
    )
    return jax.shard_map(
        per_device,
        mesh=mesh,
        in_specs=placed,
        out_specs=P(("sp", "fs", "tp"), None),
        check_vma=False,
    )
```

profile of v0, /device:TPU:0, one launch (start us, length us, event | category | flops | bytes accessed | tf_op | source)
XLA Modules:
  0.0 240.4 jit_solution(6363466625994924924)
XLA Ops:
  6.5 1.6 fusion.3
  8.1 17.7 %all_gather.30 = bf16[2048,128]{1,0:T(8,128)(2,1)S(1)} all-gather(bf16[512,128]{1,0:T(8,128)(2,1)} %param.25), channel_id=1, replica_groups=mesh['sp'=4,'fs'=4,'tp'=2] {'sp'}, dimensions={0}, use_global_device_ids=true | all-gather | bytes 655360 | tf_op jit(solution)/shard_map/all_gather | solution.py:90
  25.9 1.7 convolution_convert_fusion.5
  27.6 16.4 %all_gather.31 = bf16[2048,128]{1,0:T(8,128)(2,1)S(1)} all-gather(bf16[512,128]{1,0:T(8,128)(2,1)S(1)} %copy-done.3), channel_id=1, replica_groups=mesh['sp'=4,'fs'=4,'tp'=2] {'sp'}, dimensions={0}, use_global_device_ids=true | all-gather | bytes 655360 | tf_op jit(solution)/shard_map/all_gather | solution.py:91
  44.5 16.2 %all_gather.32 = bf16[2048,128]{1,0:T(8,128)(2,1)S(1)} all-gather(bf16[512,128]{1,0:T(8,128)(2,1)S(1)} %copy-done.4), channel_id=1, replica_groups=mesh['sp'=4,'fs'=4,'tp'=2] {'sp'}, dimensions={0}, use_global_device_ids=true | all-gather | bytes 655360 | tf_op jit(solution)/shard_map/all_gather | solution.py:92
  61.2 15.1 %all_gather.33 = bf16[2048,128]{1,0:T(8,128)(2,1)S(1)} all-gather(bf16[512,128]{1,0:T(8,128)(2,1)S(1)} %copy-done.5), channel_id=1, replica_groups=mesh['sp'=4,'fs'=4,'tp'=2] {'sp'}, dimensions={0}, use_global_device_ids=true | all-gather | bytes 655360 | tf_op jit(solution)/shard_map/all_gather | solution.py:93
  76.9 15.3 %all_gather.34 = bf16[2048,128]{1,0:T(8,128)(2,1)S(1)} all-gather(bf16[512,128]{1,0:T(8,128)(2,1)S(1)} %copy-done.6), channel_id=1, replica_groups=mesh['sp'=4,'fs'=4,'tp'=2] {'sp'}, dimensions={0}, use_global_device_ids=true | all-gather | bytes 655360 | tf_op jit(solution)/shard_map/all_gather | solution.py:94
  92.8 4.2 %collective-permute-start = (bf16[30,640]{1,0:T(8,128)(2,1)S(1)}, bf16[30,640]{1,0:T(8,128)(2,1)S(1)}, u32[]{:S(2)}, u32[]{:S(2)}) collective-permute-start(bf16[30,640]{1,0:T(8,128)(2,1)S(1)} %constant_dynamic-update-slice_fusion), channel_id=1, source_target_pairs={{0,8},{8,16},{16,24},{1,9},{9,17},{17,25},{2,10},{10,18},{18,26},{... | collective-permute-start | bytes 115208 | tf_op jit(solution)/shard_map/ppermute | solution.py:20
  99.5 9.8 %all-reduce = f32[8]{0:T(128)S(1)} all-reduce(f32[8]{0:T(128)S(1)} %dynamic-update-slice), channel_id=2, replica_groups=mesh['sp'=4,'fs'=4,'tp'=2] {'sp'}, use_global_device_ids=true, to_apply=%add | all-reduce | flops 8 | bytes 64
  109.6 15.6 %all_gather.38 = bf16[2048,128]{1,0:T(8,128)(2,1)} all-gather(bf16[512,128]{1,0:T(8,128)(2,1)S(1)} %copy-done.7), channel_id=1, replica_groups=mesh['sp'=4,'fs'=4,'tp'=2] {'sp'}, dimensions={0}, use_global_device_ids=true | all-gather | bytes 655360 | tf_op jit(solution)/shard_map/all_gather | solution.py:95
  125.2 15.9 %all_gather.35 = bf16[2048,128]{1,0:T(8,128)(2,1)S(1)} all-gather(bf16[512,128]{1,0:T(8,128)(2,1)S(1)} %copy-done.8), channel_id=1, replica_groups=mesh['sp'=4,'fs'=4,'tp'=2] {'sp'}, dimensions={0}, use_global_device_ids=true | all-gather | bytes 655360 | tf_op jit(solution)/shard_map/all_gather | solution.py:96
  141.1 15.3 %all_gather.39 = bf16[2048,128]{1,0:T(8,128)(2,1)S(1)} all-gather(bf16[512,128]{1,0:T(8,128)(2,1)S(1)} %copy-done.9), channel_id=1, replica_groups=mesh['sp'=4,'fs'=4,'tp'=2] {'sp'}, dimensions={0}, use_global_device_ids=true | all-gather | bytes 655360 | tf_op jit(solution)/shard_map/all_gather | solution.py:97
  157.2 0.7 copy.91
  159.3 0.7 slice_reduce_fusion.1
  163.4 2.9 %while.13 = (s32[]{:T(128)}, f32[2,64,128]{2,1,0:T(8,128)S(1)}, f32[4,2,64,128]{3,2,1,0:T(8,128)}, f32[4,2]{1,0:T(4,128)S(1)}, f32[4,2,64,128]{3,2,1,0:T(8,128)S(1)}, /*index=5*/s32[]{:T(128)}, s32[]{:T(128)}) while((s32[]{:T(128)}, f32[2,64,128]{2,1,0:T(8,128)S(1)}, f32[4,2,64,128]{3,2,1,0:T(8,128)}, f32[4,2]{1,0:T(4,128)S(1)}, ...), condition=%wide.region_7.8_spmd.clone, body=%wide.region_6.7_spmd.clone.sunk | while | flops 65539 | bytes 327812 | solution.py:158
  164.8 0.6 bitcast_dynamic-update-slice_fusion.2
  165.6 0.6 bitcast_dynamic-update-slice_fusion.2
  166.3 13.3 %all-gather.1 = bf16[8,64,128]{2,1,0:T(8,128)(2,1)S(1)} all-gather(bf16[2,64,128]{2,1,0:T(8,128)(2,1)S(1)} %convert_element_type.74), channel_id=3, replica_groups=mesh['sp'=4,'fs'=4,'tp'=2] {'sp'}, dimensions={0}, use_global_device_ids=true | all-gather | bytes 163840 | tf_op jit(solution)/shard_map/all_gather | solution.py:187
  179.7 1.0 fusion.35
  180.7 1.5 fusion.7
  182.2 1.7 fusion.9
  185.0 11.8 %all-reduce.1 = (f32[256]{0:T(256)S(1)}, f32[256]{0:T(256)S(1)}, f32[256]{0:T(256)S(1)}) all-reduce(f32[256]{0:T(256)S(1)} %copy-done.11, f32[256]{0:T(256)S(1)} %copy-done.10, f32[256]{0:T(256)S(1)} %get-tuple-element.99), channel_id=1, replica_groups=mesh['sp'=4,'fs'=4,'tp'=2] {'fs','tp'}, use_global_device_ids=true, to_apply=%region_4.5 | all-reduce | flops 768 | bytes 6144 | tf_op jit(solution)/shard_map/psum | solution.py:175
  197.4 1.5 fusion.2
  198.9 34.6 %reduce-scatter.2.cloned.1.call-done = bf16[32,2048]{1,0:T(8,128)(2,1)} async-done(((bf16[256,2048]{1,0:T(8,128)(2,1)}), bf16[32,2048]{1,0:T(8,128)(2,1)}) %reduce-scatter.2.cloned.1.call-update) | async-done | bytes 131088 | tf_op jit(solution)/shard_map/reduce_scatter | solution.py:212
  (144 shorter events, 12.8 us)
Async XLA Ops:
  6.5 90.6 %copy-start = (bf16[2048,16]{0,1:T(8,128)(2,1)S(1)}, bf16[2048,16]{0,1:T(8,128)(2,1)}, u32[]{:S(2)}) copy-start(bf16[2048,16]{0,1:T(8,128)(2,1)} %param.31) | copy-start | bytes 196612
  6.5 21.1 %copy-start.3 = (bf16[512,128]{1,0:T(8,128)(2,1)S(1)}, bf16[512,128]{1,0:T(8,128)(2,1)}, u32[]{:S(2)}) copy-start(bf16[512,128]{1,0:T(8,128)(2,1)} %param.26) | copy-start | bytes 393220
  6.5 227.0 %reduce-scatter.2.cloned.1.call-start = ((), (), s32[]{:S(2)}) async-start(), calls=%async_computation.1 | async-start | bytes 1179648 | tf_op jit(solution)/shard_map/reduce_scatter | solution.py:212
  8.1 35.9 %copy-start.1 = (bf16[256,2048]{1,0:T(8,128)(2,1)S(1)}, bf16[256,2048]{1,0:T(8,128)(2,1)}, u32[]{:S(2)}) copy-start(bf16[256,2048]{1,0:T(8,128)(2,1)} %param.23) | copy-start | bytes 3145732
  8.1 35.9 %copy-start.23 = (f32[2048]{0:T(1024)S(1)}, f32[2048]{0:T(1024)}, u32[]{:S(2)}) copy-start(f32[2048]{0:T(1024)} %param.24) | copy-start | bytes 24580
  8.1 89.0 %copy-start.17 = (f32[256]{0:T(256)}, f32[256]{0:T(256)S(1)}, u32[]{:S(2)}) copy-start(f32[256]{0:T(256)S(1)} %add_rsqrt_fusion.2) | copy-start | bytes 3076
  27.6 16.9 %copy-start.4 = (bf16[512,128]{1,0:T(8,128)(2,1)S(1)}, bf16[512,128]{1,0:T(8,128)(2,1)}, u32[]{:S(2)}) copy-start(bf16[512,128]{1,0:T(8,128)(2,1)} %param.28) | copy-start | bytes 393220
  44.5 16.7 %copy-start.5 = (bf16[512,128]{1,0:T(8,128)(2,1)S(1)}, bf16[512,128]{1,0:T(8,128)(2,1)}, u32[]{:S(2)}) copy-start(bf16[512,128]{1,0:T(8,128)(2,1)} %param.29) | copy-start | bytes 393220
  61.2 15.7 %copy-start.6 = (bf16[512,128]{1,0:T(8,128)(2,1)S(1)}, bf16[512,128]{1,0:T(8,128)(2,1)}, u32[]{:S(2)}) copy-start(bf16[512,128]{1,0:T(8,128)(2,1)} %param.30) | copy-start | bytes 393220
  76.9 20.2 %copy-start.25 = (f32[2]{0:T(128)S(1)}, f32[2]{0:T(128)}, u32[]{:S(2)}) copy-start(f32[2]{0:T(128)} %param.33) | copy-start | bytes 28
  92.2 5.8 %copy-start.26 = (u32[32]{0:T(128)S(1)}, u32[32]{0:T(128)}, u32[]{:S(2)}) copy-start(u32[32]{0:T(128)} %constant.87) | copy-start | bytes 388
  92.2 17.4 %copy-start.7 = (bf16[512,128]{1,0:T(8,128)(2,1)S(1)}, bf16[512,128]{1,0:T(8,128)(2,1)}, u32[]{:S(2)}) copy-start(bf16[512,128]{1,0:T(8,128)(2,1)} %param.27) | copy-start | bytes 393220
  92.7 32.5 %copy-start.8 = (bf16[512,128]{1,0:T(8,128)(2,1)S(1)}, bf16[512,128]{1,0:T(8,128)(2,1)}, u32[]{:S(2)}) copy-start(bf16[512,128]{1,0:T(8,128)(2,1)} %param.41) | copy-start | bytes 393220
  92.7 48.4 %copy-start.9 = (bf16[512,128]{1,0:T(8,128)(2,1)S(1)}, bf16[512,128]{1,0:T(8,128)(2,1)}, u32[]{:S(2)}) copy-start(bf16[512,128]{1,0:T(8,128)(2,1)} %param.42) | copy-start | bytes 393220
  92.8 65.6 %collective-permute-start = (bf16[30,640]{1,0:T(8,128)(2,1)S(1)}, bf16[30,640]{1,0:T(8,128)(2,1)S(1)}, u32[]{:S(2)}, u32[]{:S(2)}) collective-permute-start(bf16[30,640]{1,0:T(8,128)(2,1)S(1)} %constant_dynamic-update-slice_fusion), channel_id=1, source_target_pairs={{0,8},{8,16},{16,24},{1,9},{9,17},{17,25},{2,10},{10,18},{18,26},{... | collective-permute-start | bytes 115208 | tf_op jit(solution)/shard_map/ppermute | solution.py:20
  97.1 60.0 %copy-start.13 = (f32[4,128]{1,0:T(4,128)S(1)}, f32[4,128]{1,0:T(4,128)}, u32[]{:S(2)}) copy-start(f32[4,128]{1,0:T(4,128)} %param.37) | copy-start | bytes 6148
  97.1 60.0 %copy-start.14 = (f32[4,128]{1,0:T(4,128)S(1)}, f32[4,128]{1,0:T(4,128)}, u32[]{:S(2)}) copy-start(f32[4,128]{1,0:T(4,128)} %param.36) | copy-start | bytes 6148
  97.1 60.0 %copy-start.15 = (f32[4,128]{1,0:T(4,128)S(1)}, f32[4,128]{1,0:T(4,128)}, u32[]{:S(2)}) copy-start(f32[4,128]{1,0:T(4,128)} %param.35) | copy-start | bytes 6148
  163.4 18.8 %copy-start.16 = (f32[2]{0:T(128)S(1)}, f32[2]{0:T(128)}, u32[]{:S(2)}) copy-start(f32[2]{0:T(128)} %get-tuple-element.81) | copy-start | bytes 28
  163.4 21.0 %copy-start.2 = (bf16[2048,128]{1,0:T(8,128)(2,1)S(1)}, bf16[2048,128]{1,0:T(8,128)(2,1)}, u32[]{:S(2)}) copy-start(bf16[2048,128]{1,0:T(8,128)(2,1)} %all_gather.38) | copy-start | bytes 1572868
  166.3 18.1 %copy-start.18 = (f32[256]{0:T(256)S(1)}, f32[256]{0:T(256)}, u32[]{:S(2)}) copy-start(f32[256]{0:T(256)} %copy-done.17) | copy-start | bytes 3076
  166.3 18.1 %copy-start.24 = (f32[2048]{0:T(1024)S(1)}, f32[2048]{0:T(1024)}, u32[]{:S(2)}) copy-start(f32[2048]{0:T(1024)} %param.24) | copy-start | bytes 24580
  183.9 12.9 %copy-start.21 = (f32[128]{0:T(128)S(1)}, f32[128]{0:T(128)}, u32[]{:S(2)}) copy-start(f32[128]{0:T(128)} %param.39) | copy-start | bytes 1540
  185.0 12.4 %copy-start.19 = (f32[128]{0:T(128)S(1)}, f32[128]{0:T(128)}, u32[]{:S(2)}) copy-start(f32[128]{0:T(128)} %param.40) | copy-start | bytes 1540
  (7 other events, 23.2 us)
Sparse Core Ops, SparseCore 0:
  199.1 34.4 reduce-scatter.1
where the time goes:
time: 241 us; the launch traced here: 240 us
  blocking collectives  162 us (67%)
  waiting for transfers between devices  34.6 us (14%)
  between operations  14.8 us (6%)
  matrix products  13.1 us (5%)
  other arithmetic  6.76 us (3%)
  local copies, waits for them, and re-layouts  4.49 us (2%)
  starting transfers between devices  4.23 us (2%)
    reduce_scatter x1, waiting for transfers between devices, per_device(): lax.psum_scatter((term + lax.dot_general(state_out, back_state, contract,...  34.6 us
    all_gather x1, blocking collectives, per_device(): lax.all_gather(conv_value, 'sp', axis=0, tiled=True)  17.7 us
    all_gather x1, blocking collectives, per_device(): lax.all_gather(conv_gate, 'sp', axis=0, tiled=True)  16.4 us
    all_gather x1, blocking collectives, per_device(): lax.all_gather(state_input, 'sp', axis=0, tiled=True)  16.2 us
    all_gather x1, blocking collectives, per_device(): lax.all_gather(conv_output, 'sp', axis=0, tiled=True)  15.9 us
    all_gather x1, blocking collectives, per_device(): lax.all_gather(mixer_gate, 'sp', axis=0, tiled=True)  15.6 us
    all_gather x1, blocking collectives, per_device(): lax.all_gather(state_read, 'sp', axis=0, tiled=True)  15.3 us
    all_gather x1, blocking collectives, per_device(): lax.all_gather(state_output, 'sp', axis=0, tiled=True)  15.3 us
  transfers between devices with their start and end apart: 2, of which 1 were waited for; matrix products, arithmetic and copies ran while one was open for 2% of the time, Pallas kernels for 0%

commit v1 on v0

--- a/solution.py
+++ b/solution.py
@@ -1,6 +1,10 @@
+import functools
+
 import jax
 import jax.numpy as jnp
 from jax import lax
+from jax.experimental import pallas as pl
+from jax.experimental.pallas import tpu as pltpu
 from jax.sharding import PartitionSpec as P
 
 C_CH = 1024
@@ -12,12 +16,6 @@
 
 
 eps_norm = 1e-06
-
-
-def shifted(block, axis, distance):
-    devices = range(lax.axis_size(axis))
-    route = [(i - distance, i) for i in devices if i - distance in devices]
-    return lax.ppermute(block, axis, route)
 
 
 def causal_valid(padded, taps):
@@ -33,8 +31,379 @@
     return result[0]
 
 
-def project(normed, weight):
-    return jnp.dot(normed, weight, preferred_element_type=jnp.float32).astype(jnp.bfloat16)
+MESH = pl.DeviceIdType.MESH
+VMEM = pl.BlockSpec(memory_space=pltpu.VMEM)
+VMEM_LIMIT = 56 * 1024 * 1024
+EDGE = 32
+PROJECTED = 6
+HALO = 5
+COLUMN_CHUNKS = 4
+
+
+def gather_kernel(n, *refs):
+    tokens, gain, steps = refs[:3]
+    parts = refs[3:11]
+    rows_out, step_out, back_conv, back_state, before = refs[11:16]
+    normed, held, edge, send_sem, recv_sem, halo_send, halo_recv = refs[16:]
+    me = lax.axis_index("sp")
+    chunks = len(parts)
+    has_left, has_right = me > 0, me < n - 1
+    barrier = pltpu.get_barrier_semaphore()
+
+    @pl.when(has_left)
+    def _():
+        pl.semaphore_signal(barrier, inc=1, device_id={"sp": me - 1}, device_id_type=MESH)
+
+    @pl.when(has_right)
+    def _():
+        pl.semaphore_signal(barrier, inc=1, device_id={"sp": me + 1}, device_id_type=MESH)
+
+    pl.semaphore_wait(barrier, jnp.minimum(me, 1) + jnp.minimum(n - 1 - me, 1))
+
+    def link(src, chunk, block, way):
+        return pltpu.make_async_remote_copy(
+            src_ref=src,
+            dst_ref=held.at[chunk, block],
+            send_sem=send_sem.at[chunk, way],
+            recv_sem=recv_sem.at[chunk, block],
+            device_id={"sp": me + 1 if way == 0 else me - 1},
+            device_id_type=MESH,
+        )
+
+    def send_own(chunk):
+        @pl.when(has_right)
+        def _():
+            link(parts[chunk], chunk, me, 0).start()
+
+        @pl.when(has_left)
+        def _():
+            link(parts[chunk], chunk, me, 1).start()
+
+    def relay(chunk):
+        def hop(d, carry):
+            for way, source, more in ((0, me - d, has_right), (1, me + d, has_left)):
+                valid = (source >= 0) if way == 0 else (source < n)
+
+                @pl.when(valid)
+                def _():
+                    copy = link(held.at[chunk, source], chunk, source, way)
+                    copy.wait_recv()
+
+                    @pl.when(more)
+                    def _():
+                        copy.wait_send()
+                        copy.start()
+
+            return carry
+
+        lax.fori_loop(1, n, hop, 0, unroll=n <= 8)
+
+    ahead = 2
+    for chunk in range(ahead):
+        send_own(chunk)
+    values = tokens[...].astype(jnp.float32)
+    scale = lax.rsqrt(jnp.mean(values * values, axis=1, keepdims=True) + eps_norm)
+    normed[...] = (values * scale * gain[...]).astype(jnp.bfloat16)
+    step_out[...] = jnp.dot(normed[...], steps[...], preferred_element_type=jnp.float32)
+    for chunk in range(chunks):
+        held[chunk, me] = parts[chunk][...]
+    rows = tokens.shape[0]
+    width = parts[0].shape[1]
+    depth = parts[0].shape[0]
+    for chunk in range(chunks):
+        if chunk + ahead < chunks:
+            send_own(chunk + ahead)
+        relay(chunk)
+        if chunk < PROJECTED:
+            whole = held[chunk].reshape(n * depth, width)
+            rows_out[chunk] = jnp.dot(
+                normed[...], whole, preferred_element_type=jnp.float32
+            ).astype(jnp.bfloat16)
+        if chunk == HALO - 1:
+            edge[...] = rows_out[:HALO, rows - EDGE :, :]
+        if chunk == HALO:
+
+            @pl.when(has_right)
+            def _():
+                halo(edge, before, halo_send, halo_recv, me + 1).start()
+
+    back_conv[...] = held[PROJECTED].reshape(n * depth, width)
+    back_state[...] = held[PROJECTED + 1].reshape(n * depth, width)
+
+    @pl.when(has_left)
+    def _():
+        halo(edge, before, halo_send, halo_recv, me + 1).wait_recv()
+
+    @pl.when(me == 0)
+    def _():
+        before[...] = jnp.zeros_like(before)
+
+    @pl.when(has_right)
+    def _():
+        halo(edge, before, halo_send, halo_recv, me + 1).wait_send()
+
+    for chunk in range(chunks):
+
+        @pl.when(has_right)
+        def _():
+            link(parts[chunk], chunk, me, 0).wait_send()
+
+        @pl.when(has_left)
+        def _():
+            link(parts[chunk], chunk, me, 1).wait_send()
+
+
+def halo(edge, before, send, recv, target):
+    return pltpu.make_async_remote_copy(
+        src_ref=edge,
+        dst_ref=before,
+        send_sem=send,
+        recv_sem=recv,
+        device_id={"sp": target},
+        device_id_type=MESH,
+    )
+
+
+def gathered_rows(tokens, gain, steps, weights):
+    n = lax.axis_size("sp")
+    rows = tokens.shape[0]
+    depth, width = weights[0].shape
+    chunks = len(weights)
+    bf16 = jnp.bfloat16
+    return pl.pallas_call(
+        functools.partial(gather_kernel, n),
+        out_shape=(
+            jax.ShapeDtypeStruct((PROJECTED, rows, width), bf16),
+            jax.ShapeDtypeStruct((rows, steps.shape[1]), jnp.float32),
+            jax.ShapeDtypeStruct((n * depth, width), bf16),
+            jax.ShapeDtypeStruct((n * depth, width), bf16),
+            jax.ShapeDtypeStruct((HALO, EDGE, width), bf16),
+        ),
+        in_specs=[VMEM] * (3 + chunks),
+        out_specs=(VMEM,) * 5,
+        scratch_shapes=[
+            pltpu.VMEM(tokens.shape, bf16),
+            pltpu.VMEM((chunks, n, depth, width), bf16),
+            pltpu.VMEM((HALO, EDGE, width), bf16),
+            pltpu.SemaphoreType.DMA((chunks, 2)),
+            pltpu.SemaphoreType.DMA((chunks, n)),
+            pltpu.SemaphoreType.DMA,
+            pltpu.SemaphoreType.DMA,
+        ],
+        compiler_params=pltpu.CompilerParams(
+            collective_id=0, has_side_effects=True, vmem_limit_bytes=VMEM_LIMIT
+        ),
+    )(tokens, gain[None, :], steps, *weights)
+
+
+def peer_id(axes, sizes, index):
+    if len(axes) == 1:
+        return {axes[0]: index}
+    return {axes[0]: index // sizes[1], axes[1]: index % sizes[1]}
+
+
+def greet(axes, sizes, me, n):
+    barrier = pltpu.get_barrier_semaphore()
+    for i in range(1, n):
+        pl.semaphore_signal(
+            barrier,
+            inc=1,
+            device_id=peer_id(axes, sizes, lax.rem(me + i, n)),
+            device_id_type=MESH,
+        )
+    pl.semaphore_wait(barrier, n - 1)
+
+
+def index_of(axes, sizes):
+    me = lax.axis_index(axes[0])
+    return me if len(axes) == 1 else me * sizes[1] + lax.axis_index(axes[1])
+
+
+def exchange_kernel(axes, sizes, count, add, *refs):
+    ins, outs, lands = refs[:count], refs[count : 2 * count], refs[2 * count : 3 * count]
+    send_sem, recv_sem = refs[3 * count :]
+    n = 1
+    for size in sizes:
+        n *= size
+    me = index_of(axes, sizes)
+    greet(axes, sizes, me, n)
+
+    def copy(k, slot, target):
+        return pltpu.make_async_remote_copy(
+            src_ref=ins[k],
+            dst_ref=lands[k].at[slot],
+            send_sem=send_sem.at[k, slot],
+            recv_sem=recv_sem.at[k, slot],
+            device_id=peer_id(axes, sizes, target),
+            device_id_type=MESH,
+        )
+
+    for i in range(1, n):
+        for k in range(count):
+            pltpu.make_async_remote_copy(
+                src_ref=ins[k],
+                dst_ref=lands[k].at[me],
+                send_sem=send_sem.at[k, lax.rem(me + i, n)],
+                recv_sem=recv_sem.at[k, me],
+                device_id=peer_id(axes, sizes, lax.rem(me + i, n)),
+                device_id_type=MESH,
+            ).start()
+    for k in range(count):
+        lands[k][me] = ins[k][...]
+    for i in range(1, n):
+        for k in range(count):
+            copy(k, lax.rem(me + n - i, n), lax.rem(me + n - i, n)).wait_recv()
+    for k in range(count):
+        if add:
+            total = lands[k][0]
+            for i in range(1, n):
+                total = total + lands[k][i]
+            outs[k][...] = total
+        else:
+            outs[k][...] = lands[k][...]
+    for i in range(1, n):
+        for k in range(count):
+            copy(k, lax.rem(me + i, n), lax.rem(me + i, n)).wait_send()
+
+
+def exchanged(arrays, axes, add, number):
+    sizes = tuple(lax.axis_size(a) for a in axes)
+    n = 1
+    for size in sizes:
+        n *= size
+    count = len(arrays)
+    out = [
+        jax.ShapeDtypeStruct(a.shape if add else (n,) + a.shape, a.dtype) for a in arrays
+    ]
+    return pl.pallas_call(
+        functools.partial(exchange_kernel, axes, sizes, count, add),
+        out_shape=tuple(out),
+        in_specs=[VMEM] * count,
+        out_specs=(VMEM,) * count,
+        scratch_shapes=[pltpu.VMEM((n,) + a.shape, a.dtype) for a in arrays]
+        + [pltpu.SemaphoreType.DMA((count, n)), pltpu.SemaphoreType.DMA((count, n))],
+        compiler_params=pltpu.CompilerParams(
+            collective_id=number, has_side_effects=True, vmem_limit_bytes=VMEM_LIMIT
+        ),
+    )(*arrays)
+
+
+def project_kernel(sizes, conv, state, back_conv, back_state, out, *scratch):
+    core_out, core_in, plane_out, plane_in, own = scratch[:5]
+    core_send, core_recv, plane_send, plane_recv = scratch[5:]
+    n_fs, n_tp = sizes
+    fs, tp = lax.axis_index("fs"), lax.axis_index("tp")
+    me = fs * n_tp + tp
+    greet(("fs", "tp"), sizes, me, n_fs * n_tp)
+    block = conv.shape[2]
+    wide = back_conv.shape[0] // COLUMN_CHUNKS
+    contract = (((1,), (1,)), ((), ()))
+
+    def term(core, j):
+        left = jnp.concatenate([conv[f, core] for f in range(n_fs)], axis=0)
+        right = jnp.concatenate([state[f, core] for f in range(n_fs)], axis=0)
+        at = pl.ds(j * wide, wide)
+        return lax.dot_general(
+            left, back_conv[at, :], contract, preferred_element_type=jnp.float32
+        ) + lax.dot_general(
+            right, back_state[at, :], contract, preferred_element_type=jnp.float32
+        )
+
+    def core_copy(step, j):
+        target = lax.rem(tp + step, n_tp)
+        return pltpu.make_async_remote_copy(
+            src_ref=core_out.at[step - 1, j],
+            dst_ref=core_in.at[step - 1, j],
+            send_sem=core_send.at[step - 1, j],
+            recv_sem=core_recv.at[step - 1, j],
+            device_id={"tp": target},
+            device_id_type=MESH,
+        )
+
+    def plane_copy(step, j):
+        target = lax.rem(fs + step, n_fs)
+        return pltpu.make_async_remote_copy(
+            src_ref=plane_out.at[target, j],
+            dst_ref=plane_in.at[step - 1, j],
+            send_sem=plane_send.at[step - 1, j],
+            recv_sem=plane_recv.at[step - 1, j],
+            device_id={"fs": target},
+            device_id_type=MESH,
+        )
+
+    def send_core(j):
+        for step in range(1, n_tp):
+            core_copy(step, j).start()
+
+    def send_plane(j):
+        for step in range(1, n_fs):
+            plane_copy(step, j).start()
+
+    for j in range(COLUMN_CHUNKS):
+        for step in range(1, n_tp):
+            core_out[step - 1, j] = term(lax.rem(tp + step, n_tp), j).astype(jnp.bfloat16)
+        if j:
+            send_core(j - 1)
+    mine = term(tp, 0)
+    send_core(COLUMN_CHUNKS - 1)
+    for j in range(COLUMN_CHUNKS):
+        total = mine
+        for step in range(1, n_tp):
+            core_copy(step, j).wait_recv()
+            total = total + core_in[step - 1, j].astype(jnp.float32)
+        for f in range(n_fs):
+            part = total[f * block : (f + 1) * block]
+            plane_out[f, j] = part.astype(jnp.bfloat16)
+
+            @pl.when(f == fs)
+            def _():
+                own[j] = part
+
+        if j + 1 < COLUMN_CHUNKS:
+            mine = term(tp, j + 1)
+        send_plane(j)
+    for j in range(COLUMN_CHUNKS):
+        total = own[j]
+        for step in range(1, n_fs):
+            plane_copy(step, j).wait_recv()
+            total = total + plane_in[step - 1, j].astype(jnp.float32)
+        out[:, j * wide : (j + 1) * wide] = total.astype(jnp.bfloat16)
+    for j in range(COLUMN_CHUNKS):
+        for step in range(1, n_tp):
+            core_copy(step, j).wait_send()
+        for step in range(1, n_fs):
+            plane_copy(step, j).wait_send()
+
+
+def projected(conv, state, back_conv, back_state):
+    n_fs, n_tp = sizes = (lax.axis_size("fs"), lax.axis_size("tp"))
+    rows, width = conv.shape
+    block = rows // (n_fs * n_tp)
+    features = back_conv.shape[0]
+    wide = features // COLUMN_CHUNKS
+    k = COLUMN_CHUNKS
+    bf16 = jnp.bfloat16
+    shaped = (n_fs, n_tp, block, width)
+    return pl.pallas_call(
+        functools.partial(project_kernel, sizes),
+        out_shape=jax.ShapeDtypeStruct((block, features), bf16),
+        in_specs=[VMEM] * 4,
+        out_specs=VMEM,
+        scratch_shapes=[
+            pltpu.VMEM((n_tp - 1, k, n_fs * block, wide), bf16),
+            pltpu.VMEM((n_tp - 1, k, n_fs * block, wide), bf16),
+            pltpu.VMEM((n_fs, k, block, wide), bf16),
+            pltpu.VMEM((n_fs - 1, k, block, wide), bf16),
+            pltpu.VMEM((k, block, wide), jnp.float32),
+            pltpu.SemaphoreType.DMA((n_tp - 1, k)),
+            pltpu.SemaphoreType.DMA((n_tp - 1, k)),
+            pltpu.SemaphoreType.DMA((n_fs - 1, k)),
+            pltpu.SemaphoreType.DMA((n_fs - 1, k)),
+        ],
+        compiler_params=pltpu.CompilerParams(
+            collective_id=4, has_side_effects=True, vmem_limit_bytes=VMEM_LIMIT
+        ),
+    )(conv.reshape(shaped), state.reshape(shaped), back_conv, back_state)
 
 
 def carry_step(state, inputs):
@@ -73,54 +442,32 @@
     groups = width_group // STATE
     per_group = heads // groups
     head_size = width_in // heads
-    values = tokens.astype(jnp.float32)
-    normed = (
-        values * lax.rsqrt(jnp.mean(values * values, axis=1, keepdims=True) + eps_norm) * norm_gain
-    ).astype(jnp.bfloat16)
-    (
-        whole_value,
-        whole_gate,
-        whole_input,
-        whole_write,
-        whole_read,
-        whole_mixer,
-        back_conv,
-        back_state,
-    ) = (
-        lax.all_gather(conv_value, "sp", axis=0, tiled=True),
-        lax.all_gather(conv_gate, "sp", axis=0, tiled=True),
-        lax.all_gather(state_input, "sp", axis=0, tiled=True),
-        lax.all_gather(write_projection, "sp", axis=0, tiled=True),
-        lax.all_gather(state_read, "sp", axis=0, tiled=True),
-        lax.all_gather(mixer_gate, "sp", axis=0, tiled=True),
-        lax.all_gather(conv_output, "sp", axis=0, tiled=True),
-        lax.all_gather(state_output, "sp", axis=0, tiled=True),
-    )
-    input_rows = project(normed, whole_input)
-    write_rows = project(normed, whole_write)
-    read_rows = project(normed, whole_read)
-    gate_z = project(normed, whole_mixer)
-    value_rows = project(normed, whole_value)
-    gate_rows = project(normed, whole_gate)
-    step_all = jnp.dot(normed, step_proj, preferred_element_type=jnp.float32)
+    projected_rows, step_all, back_conv, back_state, before = gathered_rows(
+        tokens,
+        norm_gain,
+        step_proj,
+        (
+            state_input,
+            write_projection,
+            state_read,
+            conv_value,
+            conv_gate,
+            mixer_gate,
+            conv_output,
+            state_output,
+        ),
+    )
+    input_rows, write_rows, read_rows, value_rows, gate_rows, gate_z = (
+        projected_rows[i] for i in range(PROJECTED)
+    )
     head_start = (lax.axis_index("fs") * lax.axis_size("tp") + lax.axis_index("tp")) * heads
     step_raw = lax.dynamic_slice_in_dim(step_all, head_start, heads, 1)
     step_size = jax.nn.softplus(step_raw + step_bias)
     log_step = -jnp.exp(decay_log) * step_size + decay_extra.T
-    edge_width = WIDE_TAPS - 1
-    tail = rows - edge_width
-    packed = jnp.concatenate(
-        [
-            value_rows[tail:],
-            gate_rows[tail:],
-            input_rows[tail:],
-            write_rows[tail:],
-            read_rows[tail:],
-        ],
-        axis=1,
-    )
-    before = shifted(packed, "sp", 1)
-    short_edge = before[edge_width - SHORT_TAPS + 1 :, 2 * channels :]
+    drop = EDGE - WIDE_TAPS + 1
+    short_edge = jnp.concatenate(
+        [before[i, EDGE - SHORT_TAPS + 1 :] for i in range(3)], axis=1
+    )
     state_row_values = jnp.concatenate([input_rows, write_rows, read_rows], axis=1)
     state_full = jnp.concatenate([short_edge, state_row_values], axis=0).astype(jnp.float32)
     state_taps = jnp.concatenate([input_taps, write_taps, fetch_kernel_coefficients], axis=1)
@@ -166,27 +513,34 @@
         + jnp.einsum("bthn,bhpn->bthp", read_heads, block_states, precision=lax.Precision.HIGHEST)
         * jnp.exp(cumul)[:, :, :, None]
     )
-    value_full = jnp.concatenate([before[:, :channels], value_rows], axis=0).astype(jnp.float32)
-    gate_full = jnp.concatenate([before[:, channels : 2 * channels], gate_rows], axis=0).astype(
+    value_full = jnp.concatenate([before[3, drop:], value_rows], axis=0).astype(jnp.float32)
+    gate_full = jnp.concatenate([before[4, drop:], gate_rows], axis=0).astype(
         jnp.float32
     )
     glu = value_full * jax.nn.sigmoid(gate_full)
     long_mix = causal_valid(glu, long_taps)
-    total_sum, total_square = lax.psum(
-        (jnp.sum(long_mix, axis=1), jnp.sum(long_mix * long_mix, axis=1)), ("fs", "tp")
-    )
+    moments = jnp.stack([jnp.sum(long_mix, axis=1), jnp.sum(long_mix * long_mix, axis=1)])
+    (moments,) = exchanged((moments,), ("fs", "tp"), True, 1)
+    total_sum, total_square = moments[0], moments[1]
     mean = total_sum / C_CH
     spread = total_square / C_CH - mean * mean
     conv_out = jax.nn.silu(
         (long_mix - mean[:, None]) * lax.rsqrt(spread + eps_norm)[:, None] * conv_gain
     ).astype(jnp.bfloat16)
-    totals = lax.all_gather(logsum[None], "sp", axis=0, tiled=True)
+    piece, totals = exchanged(
+        (
+            state_end.astype(jnp.bfloat16),
+            jnp.broadcast_to(logsum[:, None], (heads, STATE)),
+        ),
+        ("sp",),
+        False,
+        3,
+    )
+    piece = piece.astype(jnp.float32)
+    totals = totals[:, :, 0]
     inclusive = jnp.cumsum(totals, axis=0)
     position = lax.axis_index("sp")
     prefix_log = lax.dynamic_index_in_dim(inclusive - totals, position, 0, keepdims=False)
-    piece = lax.all_gather(state_end[None].astype(jnp.bfloat16), "sp", axis=0, tiled=True).astype(
-        jnp.float32
-    )
     count = piece.shape[0]
     order = jnp.arange(count, dtype=jnp.int32)
     live = (order < position)[:, None]
@@ -201,23 +555,14 @@
         * start_decay[:, :, :, None]
     )
     gated = outputs.reshape(rows, width_in) * jax.nn.silu(gate_z.astype(jnp.float32))
-    quadratic_total = lax.psum(jnp.sum(gated * gated, axis=1), ("fs", "tp"))
+    (quadratic_total,) = exchanged(
+        (jnp.sum(gated * gated, axis=1)[None, :],), ("fs", "tp"), True, 2
+    )
+    quadratic_total = quadratic_total[0]
     state_out = (
         gated * lax.rsqrt(quadratic_total / D_INNER + eps_norm)[:, None] * state_gain
     ).astype(jnp.bfloat16)
-    contract = (((1,), (1,)), ((), ()))
-    out_rows = rows // (lax.axis_size("fs") * lax.axis_size("tp"))
-    conv_part = lax.slice_in_dim(conv_out, 0, out_rows * lax.axis_size(("fs", "tp")), axis=0)
-    term = lax.dot_general(conv_part, back_conv, contract, preferred_element_type=jnp.float32)
-    return lax.psum_scatter(
-        (
-            term
-            + lax.dot_general(state_out, back_state, contract, preferred_element_type=jnp.float32)
-        ).astype(jnp.bfloat16),
-        ("fs", "tp"),
-        scatter_dimension=0,
-        tiled=True,
-    )
+    return projected(conv_out, state_out, back_conv, back_state)
 
 
 def solution(mesh):

time: 241 us -> 140 us (0.58)
  blocking collectives: 162 us -> 0 us
  Pallas kernels: 0 us -> 112 us
  waiting for transfers between devices: 34.6 us -> 0 us
  between operations: 14.8 us -> 0.31 us
  local copies, waits for them, and re-layouts: 4.49 us -> 13 us
  matrix products: 13.1 us -> 7.67 us
  starting transfers between devices: 4.23 us -> 0 us
    all_gather x9 -> x0, blocking collectives: 141 us -> none  [the longest x1 17.7 us: per_device(): lax.all_gather(conv_value, 'sp', axis=0, tiled=True)]
    pallas_call x0 -> x5, Pallas kernels: none -> 112 us  [the longest x1 79.5 us: gathered_rows(): pl.pallas_call(functools.partial(gather_kernel, n), out_shape=(jax.ShapeD...]
    reduce_scatter x1 -> x0, waiting for transfers between devices: 34.6 us -> none  [per_device(): lax.psum_scatter((term + lax.dot_general(state_out, back_state, contract,...]
    psum x1 -> x0, blocking collectives: 11.8 us -> none  [per_device(): lax.psum((jnp.sum(long_mix, axis=1), jnp.sum(long_mix * long_mix, axis=1)...]
    unnamed x1 -> x0, blocking collectives: 9.77 us -> none
    unnamed x67 -> x32, local copies, waits for them, and re-layouts: 1.21 us -> 8.18 us
    dot_general x9 -> x0, matrix products: 6.83 us -> none  [the longest x6 4.31 us: project(): jnp.dot(normed, weight, preferred_element_type=jnp.float32)]
    ppermute x1 -> x0, starting transfers between devices: 4.23 us -> none  [shifted(): return lax.ppermute(block, axis, route)]
  transfers between devices with their start and end apart: 2 -> 0, of which waited for: 1 -> 0; matrix products, arithmetic and copies ran while one was open for 2% -> 0% of each run, Pallas kernels for 0% -> 0%
where the time goes in v1:
time: 140 us; the launch traced here: 139 us
  Pallas kernels  112 us (80%)
  local copies, waits for them, and re-layouts  13 us (9%)
  matrix products  7.67 us (5%)
  other arithmetic  5.75 us (4%)
    pallas_call x1, Pallas kernels, gathered_rows(): pl.pallas_call(functools.partial(gather_kernel, n), out_shape=(jax.ShapeD...  79.5 us
    pallas_call x3, Pallas kernels, exchanged(): pl.pallas_call(functools.partial(exchange_kernel, axes, sizes, count, add...  19.5 us
    pallas_call x1, Pallas kernels, projected(): pl.pallas_call(functools.partial(project_kernel, sizes), out_shape=jax.Sh...  13.3 us
    unnamed x32, local copies, waits for them, and re-layouts  8.18 us
    conv_general_dilated x2, matrix products, causal_valid(): lax.conv_general_dilated(padded[None], taps[:, None, :], window_strides=(...  3.35 us

profile of v1, /device:TPU:0, one launch (start us, length us, event | category | flops | bytes accessed | tf_op | source)
XLA Modules:
  0.0 139.2 jit_solution(12975188056263555901)
XLA Ops:
  0.0 0.7 copy-done
  0.7 0.6 copy-done.13
  1.5 0.6 copy-done.5
  2.3 0.7 copy-done.2
  3.0 1.0 copy.68.refs_2_
  4.0 79.5 %shard_map.199 = (bf16[6,256,128]{2,1,0:T(8,128)(2,1)}, f32[256,16]{1,0:T(8,128)}, bf16[2048,128]{1,0:T(8,128)(2,1)}, bf16[2048,128]{1,0:T(8,128)(2,1)}, bf16[5,32,128]{2,1,0:T(8,128)(2,1)}) custom-call(bf16[256,2048]{1,0:T(8,128)(2,1)} %refs_0_.1, f32[1,2048]{1,0:T(1,128)} %bitcast.95, bf16[2048,16]{1,0:T(8,128)(2,1)} %copy.68.refs_2_, ...), custom_call_target="tpu_custom_call" | custom-call | tf_op jit(solution)/shard_map/pallas_call | solution.py:173
  83.5 0.7 slice_bitcast_fusion.5
  84.2 0.7 fusion.35
  84.9 1.0 slice_convert_fusion
  86.0 0.8 copy-done.1
  88.3 2.8 %fusion.33 = (f32[256]{0:T(256)S(1)}, f32[256]{0:T(256)S(1)}, f32[1,256,128]{2,0,1:T(1,128)S(1)}) fusion(f32[31,1,128]{2,0,1:T(8,128)S(1)} %bitcast.83, f32[1,286,128]{2,1,0:T(8,128)S(1)} %divide_multiply_fusion), kind=kOutput, calls=%fused_computation.73 | convolution fusion | flops 12287488 | bytes 295424 | tf_op jit(solution)/shard_map/conv_general_dilated | solution.py:22
  91.6 6.0 %shard_map.200 = f32[2,256]{1,0:T(2,128)} custom-call(f32[2,256]{1,0:T(2,128)} %pad_maximum_fusion.1.refs_0_), custom_call_target="tpu_custom_call" | custom-call | tf_op jit(solution)/shard_map/pallas_call | solution.py:278
  102.7 7.6 %shard_map.201 = (bf16[4,2,64,128]{3,2,1,0:T(8,128)(2,1)}, f32[4,2,128]{2,1,0:T(2,128)}) custom-call(bf16[2,64,128]{2,1,0:T(8,128)(2,1)} %convert_element_type.49.refs_0_, f32[2,128]{1,0:T(2,128)} %broadcast_in_dim.104.refs_1_), custom_call_target="tpu_custom_call" | custom-call | tf_op jit(solution)/shard_map/pallas_call | solution.py:278
  110.3 0.7 copy-done.4
  111.5 1.3 fusion.25
  112.8 0.9 multiply_reduce_fusion
  113.8 0.6 broadcast_in_dim.106.refs_0_
  114.4 5.9 %shard_map.202 = f32[1,256]{1,0:T(1,128)} custom-call(f32[1,256]{1,0:T(1,128)} %broadcast_in_dim.106.refs_0_), custom_call_target="tpu_custom_call" | custom-call | tf_op jit(solution)/shard_map/pallas_call | solution.py:278
  120.3 0.7 multiply_reduce_fusion.3
  121.2 0.6 copy-done.10
  121.9 0.8 multiply_convert_fusion.1.conv
  123.6 0.7 multiply_convert_fusion.state
  124.3 13.3 %shard_map.203 = bf16[32,2048]{1,0:T(8,128)(2,1)} custom-call(bf16[4,2,32,128]{3,2,1,0:T(8,128)(2,1)} %multiply_convert_fusion.1.conv, bf16[4,2,32,128]{3,2,1,0:T(8,128)(2,1)} %multiply_convert_fusion.state, bf16[2048,128]{1,0:T(8,128)(2,1)} %get-tuple-element.47.back_conv, bf16[2048,128]{1,0:T(8,128)(2,1)} %get-tuple-element.48.back_state), custom_call_target="tpu_custom_call" | custom-call | tf_op jit(solution)/shard_map/pallas_call | solution.py:387
  137.6 1.6 %copy.119 = bf16[32,2048]{1,0:T(8,128)(2,1)} copy(bf16[32,2048]{1,0:T(8,128)(2,1)} %shard_map.203) | data formatting | bytes 262144
  (82 shorter events, 9.2 us)
Async XLA Ops:
  0.0 0.7 copy-start
  0.0 1.4 copy-start.8
  0.7 0.7 copy-start.13
  0.7 0.7 copy-start.7
  0.7 0.7 copy-start.6
  1.4 0.7 copy-start.5
  2.1 0.8 copy-start.2
  86.0 0.9 copy-start.1
  86.0 0.9 copy-start.9
  110.3 0.7 copy-start.4
  111.5 1.3 copy-start.12
  113.7 6.6 %copy-start.3 = (f32[2,256]{1,0:T(2,128)S(1)}, f32[2,256]{1,0:T(2,128)}, u32[]{:S(2)}) copy-start(f32[2,256]{1,0:T(2,128)} %shard_map.200) | copy-start | bytes 6148
  121.2 0.7 copy-start.10
  122.9 0.7 copy-start.11

commit v2 on v1

--- a/solution.py
+++ b/solution.py
@@ -98,7 +98,7 @@
 
         lax.fori_loop(1, n, hop, 0, unroll=n <= 8)
 
-    ahead = 2
+    ahead = chunks
     for chunk in range(ahead):
         send_own(chunk)
     values = tokens[...].astype(jnp.float32)
@@ -219,41 +219,50 @@
     return me if len(axes) == 1 else me * sizes[1] + lax.axis_index(axes[1])
 
 
-def exchange_kernel(axes, sizes, count, add, *refs):
+def exchange_kernel(groups, *refs):
+    count = len(groups)
     ins, outs, lands = refs[:count], refs[count : 2 * count], refs[2 * count : 3 * count]
-    send_sem, recv_sem = refs[3 * count :]
-    n = 1
-    for size in sizes:
-        n *= size
-    me = index_of(axes, sizes)
-    greet(axes, sizes, me, n)
-
-    def copy(k, slot, target):
+    sems = refs[3 * count :]
+    barrier = pltpu.get_barrier_semaphore()
+    greeted = set()
+    expected = 0
+    for axes, sizes, n, add in groups:
+        if axes in greeted:
+            continue
+        greeted.add(axes)
+        me = index_of(axes, sizes)
+        for i in range(1, n):
+            pl.semaphore_signal(
+                barrier,
+                inc=1,
+                device_id=peer_id(axes, sizes, lax.rem(me + i, n)),
+                device_id_type=MESH,
+            )
+        expected += n - 1
+    pl.semaphore_wait(barrier, expected)
+
+    def copy(k, slot, land, target):
+        axes, sizes, n, add = groups[k]
         return pltpu.make_async_remote_copy(
             src_ref=ins[k],
-            dst_ref=lands[k].at[slot],
-            send_sem=send_sem.at[k, slot],
-            recv_sem=recv_sem.at[k, slot],
+            dst_ref=lands[k].at[land],
+            send_sem=sems[2 * k].at[slot],
+            recv_sem=sems[2 * k + 1].at[land],
             device_id=peer_id(axes, sizes, target),
             device_id_type=MESH,
         )
 
-    for i in range(1, n):
-        for k in range(count):
-            pltpu.make_async_remote_copy(
-                src_ref=ins[k],
-                dst_ref=lands[k].at[me],
-                send_sem=send_sem.at[k, lax.rem(me + i, n)],
-                recv_sem=recv_sem.at[k, me],
-                device_id=peer_id(axes, sizes, lax.rem(me + i, n)),
-                device_id_type=MESH,
-            ).start()
-    for k in range(count):
+    for k, (axes, sizes, n, add) in enumerate(groups):
+        me = index_of(axes, sizes)
+        for i in range(1, n):
+            target = lax.rem(me + i, n)
+            copy(k, target, me, target).start()
+    for k, (axes, sizes, n, add) in enumerate(groups):
+        me = index_of(axes, sizes)
         lands[k][me] = ins[k][...]
-    for i in range(1, n):
-        for k in range(count):
-            copy(k, lax.rem(me + n - i, n), lax.rem(me + n - i, n)).wait_recv()
-    for k in range(count):
+        for i in range(1, n):
+            source = lax.rem(me + n - i, n)
+            copy(k, source, source, source).wait_recv()
         if add:
             total = lands[k][0]
             for i in range(1, n):
@@ -261,40 +270,75 @@
             outs[k][...] = total
         else:
             outs[k][...] = lands[k][...]
-    for i in range(1, n):
-        for k in range(count):
-            copy(k, lax.rem(me + i, n), lax.rem(me + i, n)).wait_send()
-
-
-def exchanged(arrays, axes, add, number):
-    sizes = tuple(lax.axis_size(a) for a in axes)
-    n = 1
-    for size in sizes:
-        n *= size
+    for k, (axes, sizes, n, add) in enumerate(groups):
+        me = index_of(axes, sizes)
+        for i in range(1, n):
+            target = lax.rem(me + i, n)
+            copy(k, target, me, target).wait_send()
+
+
+def exchanged(arrays, plans, number):
+    groups, out, lands, sems = [], [], [], []
+    for array, (axes, add) in zip(arrays, plans):
+        sizes = tuple(lax.axis_size(a) for a in axes)
+        n = 1
+        for size in sizes:
+            n *= size
+        groups.append((axes, sizes, n, add))
+        shape = (n,) + array.shape
+        out.append(jax.ShapeDtypeStruct(array.shape if add else shape, array.dtype))
+        lands.append(pltpu.VMEM(shape, array.dtype))
+        sems += [pltpu.SemaphoreType.DMA((n,)), pltpu.SemaphoreType.DMA((n,))]
     count = len(arrays)
-    out = [
-        jax.ShapeDtypeStruct(a.shape if add else (n,) + a.shape, a.dtype) for a in arrays
-    ]
     return pl.pallas_call(
-        functools.partial(exchange_kernel, axes, sizes, count, add),
+        functools.partial(exchange_kernel, tuple(groups)),
         out_shape=tuple(out),
         in_specs=[VMEM] * count,
         out_specs=(VMEM,) * count,
-        scratch_shapes=[pltpu.VMEM((n,) + a.shape, a.dtype) for a in arrays]
-        + [pltpu.SemaphoreType.DMA((count, n)), pltpu.SemaphoreType.DMA((count, n))],
+        scratch_shapes=lands + sems,
         compiler_params=pltpu.CompilerParams(
             collective_id=number, has_side_effects=True, vmem_limit_bytes=VMEM_LIMIT
         ),
     )(*arrays)
 
 
-def project_kernel(sizes, conv, state, back_conv, back_state, out, *scratch):
+def project_kernel(sizes, conv, gated, square, gain, back_conv, back_state, out, *scratch):
     core_out, core_in, plane_out, plane_in, own = scratch[:5]
-    core_send, core_recv, plane_send, plane_recv = scratch[5:]
+    core_send, core_recv, plane_send, plane_recv = scratch[5:9]
+    state, squares, square_send, square_recv = scratch[9:]
     n_fs, n_tp = sizes
     fs, tp = lax.axis_index("fs"), lax.axis_index("tp")
     me = fs * n_tp + tp
-    greet(("fs", "tp"), sizes, me, n_fs * n_tp)
+    n = n_fs * n_tp
+    greet(("fs", "tp"), sizes, me, n)
+
+    def square_copy(slot, land, target):
+        return pltpu.make_async_remote_copy(
+            src_ref=square,
+            dst_ref=squares.at[land],
+            send_sem=square_send.at[slot],
+            recv_sem=square_recv.at[land],
+            device_id=peer_id(("fs", "tp"), sizes, target),
+            device_id_type=MESH,
+        )
+
+    for i in range(1, n):
+        target = lax.rem(me + i, n)
+        square_copy(target, me, target).start()
+    squares[me] = square[...]
+    for i in range(1, n):
+        source = lax.rem(me + n - i, n)
+        square_copy(source, source, source).wait_recv()
+    whole = squares[0]
+    for i in range(1, n):
+        whole = whole + squares[i]
+    factor = lax.rsqrt(whole / D_INNER + eps_norm)
+    factor = jnp.broadcast_to(factor, (8, factor.shape[1])).T[:, :1]
+    rows = conv.shape[2]
+    for f in range(n_fs):
+        for c in range(n_tp):
+            at = (f * n_tp + c) * rows
+            state[f, c] = (gated[f, c] * factor[at : at + rows] * gain[...]).astype(jnp.bfloat16)
     block = conv.shape[2]
     wide = back_conv.shape[0] // COLUMN_CHUNKS
     contract = (((1,), (1,)), ((), ()))
@@ -368,6 +412,9 @@
             plane_copy(step, j).wait_recv()
             total = total + plane_in[step - 1, j].astype(jnp.float32)
         out[:, j * wide : (j + 1) * wide] = total.astype(jnp.bfloat16)
+    for i in range(1, n):
+        target = lax.rem(me + i, n)
+        square_copy(target, me, target).wait_send()
     for j in range(COLUMN_CHUNKS):
         for step in range(1, n_tp):
             core_copy(step, j).wait_send()
@@ -375,7 +422,7 @@
             plane_copy(step, j).wait_send()
 
 
-def projected(conv, state, back_conv, back_state):
+def projected(conv, gated, square, gain, back_conv, back_state):
     n_fs, n_tp = sizes = (lax.axis_size("fs"), lax.axis_size("tp"))
     rows, width = conv.shape
     block = rows // (n_fs * n_tp)
@@ -387,7 +434,7 @@
     return pl.pallas_call(
         functools.partial(project_kernel, sizes),
         out_shape=jax.ShapeDtypeStruct((block, features), bf16),
-        in_specs=[VMEM] * 4,
+        in_specs=[VMEM] * 6,
         out_specs=VMEM,
         scratch_shapes=[
             pltpu.VMEM((n_tp - 1, k, n_fs * block, wide), bf16),
@@ -399,11 +446,22 @@
             pltpu.SemaphoreType.DMA((n_tp - 1, k)),
             pltpu.SemaphoreType.DMA((n_fs - 1, k)),
             pltpu.SemaphoreType.DMA((n_fs - 1, k)),
+            pltpu.VMEM(shaped, bf16),
+            pltpu.VMEM((n_fs * n_tp, 1, rows), jnp.float32),
+            pltpu.SemaphoreType.DMA((n_fs * n_tp,)),
+            pltpu.SemaphoreType.DMA((n_fs * n_tp,)),
         ],
         compiler_params=pltpu.CompilerParams(
             collective_id=4, has_side_effects=True, vmem_limit_bytes=VMEM_LIMIT
         ),
-    )(conv.reshape(shaped), state.reshape(shaped), back_conv, back_state)
+    )(
+        conv.reshape(shaped),
+        gated.reshape(shaped),
+        square[None, :],
+        gain[None, :],
+        back_conv,
+        back_state,
+    )
 
 
 def carry_step(state, inputs):
@@ -520,22 +578,21 @@
     glu = value_full * jax.nn.sigmoid(gate_full)
     long_mix = causal_valid(glu, long_taps)
     moments = jnp.stack([jnp.sum(long_mix, axis=1), jnp.sum(long_mix * long_mix, axis=1)])
-    (moments,) = exchanged((moments,), ("fs", "tp"), True, 1)
+    moments, piece, totals = exchanged(
+        (
+            moments,
+            state_end.astype(jnp.bfloat16),
+            jnp.broadcast_to(logsum[:, None], (heads, STATE)),
+        ),
+        ((("fs", "tp"), True), (("sp",), False), (("sp",), False)),
+        1,
+    )
     total_sum, total_square = moments[0], moments[1]
     mean = total_sum / C_CH
     spread = total_square / C_CH - mean * mean
     conv_out = jax.nn.silu(
         (long_mix - mean[:, None]) * lax.rsqrt(spread + eps_norm)[:, None] * conv_gain
     ).astype(jnp.bfloat16)
-    piece, totals = exchanged(
-        (
-            state_end.astype(jnp.bfloat16),
-            jnp.broadcast_to(logsum[:, None], (heads, STATE)),
-        ),
-        ("sp",),
-        False,
-        3,
-    )
     piece = piece.astype(jnp.float32)
     totals = totals[:, :, 0]
     inclusive = jnp.cumsum(totals, axis=0)
@@ -555,14 +612,9 @@
         * start_decay[:, :, :, None]
     )
     gated = outputs.reshape(rows, width_in) * jax.nn.silu(gate_z.astype(jnp.float32))
-    (quadratic_total,) = exchanged(
-        (jnp.sum(gated * gated, axis=1)[None, :],), ("fs", "tp"), True, 2
-    )
-    quadratic_total = quadratic_total[0]
-    state_out = (
-        gated * lax.rsqrt(quadratic_total / D_INNER + eps_norm)[:, None] * state_gain
-    ).astype(jnp.bfloat16)
-    return projected(conv_out, state_out, back_conv, back_state)
+    return projected(
+        conv_out, gated, jnp.sum(gated * gated, axis=1), state_gain, back_conv, back_state
+    )
 
 
 def solution(mesh):

time: 140 us -> 132 us (0.943)
  Pallas kernels: 112 us -> 106 us
    pallas_call x3 -> x1, Pallas kernels: 19.5 us -> 9.13 us  [exchanged(): pl.pallas_call(functools.partial(exchange_kernel, tuple(groups)), out_sha...]
    pallas_call x1, Pallas kernels: 13.3 us -> 16.4 us  [projected(): pl.pallas_call(functools.partial(project_kernel, sizes), out_shape=jax.Sh...]
    convert_element_type x2 -> x0, other arithmetic: 1.5 us -> none  [the longest x1 0.78 us: per_device(): conv_out = jax.nn.silu((long_mix - mean[:, None]) * lax.rsqrt(spread + ep...]
    unnamed x32 -> x30, local copies, waits for them, and re-layouts: 8.18 us -> 8.09 us
where the time goes in v2:
time: 132 us; the launch traced here: 131 us
  Pallas kernels  106 us (80%)
  local copies, waits for them, and re-layouts  12.9 us (10%)
  matrix products  7.66 us (6%)
  other arithmetic  4.39 us (3%)
    pallas_call x1, Pallas kernels, gathered_rows(): pl.pallas_call(functools.partial(gather_kernel, n), out_shape=(jax.ShapeD...  80.5 us
    pallas_call x1, Pallas kernels, projected(): pl.pallas_call(functools.partial(project_kernel, sizes), out_shape=jax.Sh...  16.4 us
    pallas_call x1, Pallas kernels, exchanged(): pl.pallas_call(functools.partial(exchange_kernel, tuple(groups)), out_sha...  9.13 us
    unnamed x30, local copies, waits for them, and re-layouts  8.09 us
    conv_general_dilated x2, matrix products, causal_valid(): lax.conv_general_dilated(padded[None], taps[:, None, :], window_strides=(...  3.35 us

profile of v2, /device:TPU:0, one launch (start us, length us, event | category | flops | bytes accessed | tf_op | source)
XLA Modules:
  0.0 131.3 jit_solution(15102876295217872041)
XLA Ops:
  0.0 0.7 copy-done
  0.7 0.6 copy-done.12
  1.5 0.6 copy-done.4
  2.3 0.7 copy-done.2
  3.0 1.0 copy.68.refs_2_
  4.0 80.5 %shard_map.199 = (bf16[6,256,128]{2,1,0:T(8,128)(2,1)}, f32[256,16]{1,0:T(8,128)}, bf16[2048,128]{1,0:T(8,128)(2,1)}, bf16[2048,128]{1,0:T(8,128)(2,1)}, bf16[5,32,128]{2,1,0:T(8,128)(2,1)}) custom-call(bf16[256,2048]{1,0:T(8,128)(2,1)} %refs_0_.1, f32[1,2048]{1,0:T(1,128)} %bitcast.96, bf16[2048,16]{1,0:T(8,128)(2,1)} %copy.68.refs_2_, ...), custom_call_target="tpu_custom_call" | custom-call | tf_op jit(solution)/shard_map/pallas_call | solution.py:173
  84.5 0.7 slice_bitcast_fusion.5
  85.2 0.7 fusion.35
  85.9 1.0 slice_convert_fusion
  87.0 0.8 copy-done.1
  88.3 0.6 broadcast_in_dim.100.refs_2_
  89.3 2.8 %fusion.33 = (f32[256]{0:T(256)S(1)}, f32[256]{0:T(256)S(1)}, f32[1,256,128]{2,0,1:T(1,128)S(1)}) fusion(f32[31,1,128]{2,0,1:T(8,128)S(1)} %bitcast.84, f32[1,286,128]{2,1,0:T(8,128)S(1)} %divide_multiply_fusion), kind=kOutput, calls=%fused_computation.72 | convolution fusion | flops 12287488 | bytes 295424 | tf_op jit(solution)/shard_map/conv_general_dilated | solution.py:22
  92.0 0.6 pad_maximum_fusion.1.refs_0_
  92.6 0.6 fusion.6
  97.0 0.6 convert_element_type.44.refs_1_
  97.6 9.1 %shard_map.200 = (f32[2,256]{1,0:T(2,128)}, bf16[4,2,64,128]{3,2,1,0:T(8,128)(2,1)}, f32[4,2,128]{2,1,0:T(2,128)}) custom-call(f32[2,256]{1,0:T(2,128)} %pad_maximum_fusion.1.refs_0_, bf16[2,64,128]{2,1,0:T(8,128)(2,1)} %convert_element_type.44.refs_1_, f32[2,128]{1,0:T(2,128)} %broadcast_in_dim.100.refs_2_), custom_call_target="tpu_custom_call" | custom-call | tf_op jit(solution)/shard_map/pallas_call | solution.py:293
  106.8 0.7 copy-done.3
  107.5 0.6 copy-done.5
  108.6 1.3 fusion.25
  109.9 0.9 multiply_reduce_fusion
  110.8 0.7 broadcast_in_dim.107.square
  112.5 0.8 multiply_multiply_fusion
  113.3 16.4 %shard_map.201 = bf16[32,2048]{1,0:T(8,128)(2,1)} custom-call(bf16[4,2,32,128]{3,2,1,0:T(8,128)(2,1)} %get-tuple-element.123.conv, f32[4,2,32,128]{3,2,1,0:T(8,128)} %get-tuple-element.122.gated, f32[1,256]{1,0:T(1,128)} %broadcast_in_dim.107.square, f32[1,128]{1,0:T(1,128)} %bitcast.103, bf16[2048,128]{1,0:T(8,128)(2,1)} %get-tuple-element.49.back_conv, ...), custom_call_target="tpu_custom_call" | custom-call | tf_op jit(solution)/shard_map/pallas_call | solution.py:434
  129.7 1.6 %copy.119 = bf16[32,2048]{1,0:T(8,128)(2,1)} copy(bf16[32,2048]{1,0:T(8,128)(2,1)} %shard_map.201) | data formatting | bytes 262144
  (76 shorter events, 6.7 us)
Async XLA Ops:
  0.0 0.7 copy-start
  0.0 1.4 %copy-start.8 = (f32[4,128]{1,0:T(4,128)S(1)}, f32[4,128]{1,0:T(4,128)}, u32[]{:S(2)}) copy-start(f32[4,128]{1,0:T(4,128)} %param.35) | copy-start | bytes 6148
  0.7 0.7 copy-start.12
  0.7 0.7 copy-start.7
  0.7 0.7 copy-start.6
  1.4 0.7 copy-start.4
  2.1 0.8 copy-start.2
  86.9 0.9 copy-start.1
  86.9 0.9 copy-start.9
  106.7 0.7 copy-start.3
  107.4 0.7 copy-start.5
  108.5 1.3 copy-start.11
  111.8 0.7 copy-start.10

commit v3 on v2

--- a/solution.py
+++ b/solution.py
@@ -79,24 +79,19 @@
         def _():
             link(parts[chunk], chunk, me, 1).start()
 
-    def relay(chunk):
-        def hop(d, carry):
-            for way, source, more in ((0, me - d, has_right), (1, me + d, has_left)):
-                valid = (source >= 0) if way == 0 else (source < n)
-
-                @pl.when(valid)
+    def hop(d, chunk):
+        for way, source, more in ((0, me - d, has_right), (1, me + d, has_left)):
+            valid = (source >= 0) if way == 0 else (source < n)
+
+            @pl.when(valid)
+            def _():
+                copy = link(held.at[chunk, source], chunk, source, way)
+                copy.wait_recv()
+
+                @pl.when(more)
                 def _():
-                    copy = link(held.at[chunk, source], chunk, source, way)
-                    copy.wait_recv()
-
-                    @pl.when(more)
-                    def _():
-                        copy.wait_send()
-                        copy.start()
-
-            return carry
-
-        lax.fori_loop(1, n, hop, 0, unroll=n <= 8)
+                    copy.wait_send()
+                    copy.start()
 
     ahead = chunks
     for chunk in range(ahead):
@@ -110,10 +105,15 @@
     rows = tokens.shape[0]
     width = parts[0].shape[1]
     depth = parts[0].shape[0]
+
+    def round_of(d, carry):
+        for chunk in range(chunks):
+            hop(d, chunk)
+        return carry
+
+    lax.fori_loop(1, n - 1, round_of, 0)
     for chunk in range(chunks):
-        if chunk + ahead < chunks:
-            send_own(chunk + ahead)
-        relay(chunk)
+        hop(n - 1, chunk)
         if chunk < PROJECTED:
             whole = held[chunk].reshape(n * depth, width)
             rows_out[chunk] = jnp.dot(

time: 132 us -> 128 us (0.970)
  Pallas kernels: 106 us -> 102 us
    pallas_call x1, Pallas kernels: 80.5 us -> 75.9 us  [gathered_rows(): pl.pallas_call(functools.partial(gather_kernel, n), out_shape=(jax.ShapeD...]
    pallas_call x1, Pallas kernels: 9.13 us -> 10.6 us  [exchanged(): pl.pallas_call(functools.partial(exchange_kernel, tuple(groups)), out_sha...]
where the time goes in v3:
time: 128 us
  Pallas kernels  102 us (80%)
  local copies, waits for them, and re-layouts  12.9 us (10%)
  matrix products  7.66 us (6%)
  other arithmetic  4.39 us (3%)
    pallas_call x1, Pallas kernels, gathered_rows(): pl.pallas_call(functools.partial(gather_kernel, n), out_shape=(jax.ShapeD...  75.9 us
    pallas_call x1, Pallas kernels, projected(): pl.pallas_call(functools.partial(project_kernel, sizes), out_shape=jax.Sh...  15.9 us
    pallas_call x1, Pallas kernels, exchanged(): pl.pallas_call(functools.partial(exchange_kernel, tuple(groups)), out_sha...  10.6 us
    unnamed x30, local copies, waits for them, and re-layouts  8.09 us
    conv_general_dilated x2, matrix products, causal_valid(): lax.conv_general_dilated(padded[None], taps[:, None, :], window_strides=(...  3.35 us

profile of v3, /device:TPU:0, one launch (start us, length us, event | category | flops | bytes accessed | tf_op | source)
XLA Modules:
  0.0 127.7 jit_solution(17198655053293111459)
XLA Ops:
  0.0 0.7 copy-done
  0.7 0.6 copy-done.12
  1.5 0.6 copy-done.4
  2.3 0.7 copy-done.2
  3.0 1.0 copy.68.refs_2_
  4.0 75.9 %shard_map.199 = (bf16[6,256,128]{2,1,0:T(8,128)(2,1)}, f32[256,16]{1,0:T(8,128)}, bf16[2048,128]{1,0:T(8,128)(2,1)}, bf16[2048,128]{1,0:T(8,128)(2,1)}, bf16[5,32,128]{2,1,0:T(8,128)(2,1)}) custom-call(bf16[256,2048]{1,0:T(8,128)(2,1)} %refs_0_.1, f32[1,2048]{1,0:T(1,128)} %bitcast.96, bf16[2048,16]{1,0:T(8,128)(2,1)} %copy.68.refs_2_, ...), custom_call_target="tpu_custom_call" | custom-call | tf_op jit(solution)/shard_map/pallas_call | solution.py:173
  79.9 0.7 slice_bitcast_fusion.5
  80.6 0.7 fusion.35
  81.4 1.0 slice_convert_fusion
  82.5 0.8 copy-done.1
  83.7 0.6 broadcast_in_dim.100.refs_2_
  84.8 2.8 %fusion.33 = (f32[256]{0:T(256)S(1)}, f32[256]{0:T(256)S(1)}, f32[1,256,128]{2,0,1:T(1,128)S(1)}) fusion(f32[31,1,128]{2,0,1:T(8,128)S(1)} %bitcast.84, f32[1,286,128]{2,1,0:T(8,128)S(1)} %divide_multiply_fusion), kind=kOutput, calls=%fused_computation.72 | convolution fusion | flops 12287488 | bytes 295424 | tf_op jit(solution)/shard_map/conv_general_dilated | solution.py:22
  87.5 0.6 pad_maximum_fusion.1.refs_0_
  88.1 0.6 fusion.6
  92.5 0.6 convert_element_type.44.refs_1_
  93.1 10.6 %shard_map.200 = (f32[2,256]{1,0:T(2,128)}, bf16[4,2,64,128]{3,2,1,0:T(8,128)(2,1)}, f32[4,2,128]{2,1,0:T(2,128)}) custom-call(f32[2,256]{1,0:T(2,128)} %pad_maximum_fusion.1.refs_0_, bf16[2,64,128]{2,1,0:T(8,128)(2,1)} %convert_element_type.44.refs_1_, f32[2,128]{1,0:T(2,128)} %broadcast_in_dim.100.refs_2_), custom_call_target="tpu_custom_call" | custom-call | tf_op jit(solution)/shard_map/pallas_call | solution.py:293
  103.7 0.7 copy-done.3
  104.4 0.6 copy-done.5
  105.5 1.3 %fusion.25 = f32[2,1,64,128]{3,1,2,0:T(1,128)S(1)} fusion(f32[4,2,1,1]{0,2,3,1:T(1,128)S(1)} %bitcast.100, bf16[4,2,64,128]{3,2,1,0:T(8,128)(2,1)} %get-tuple-element.48), kind=kOutput, calls=%fused_computation.45 | convolution fusion | flops 786432 | bytes 196640 | tf_op jit(solution)/shard_map/kh,khpn->hpn/dot_general | solution.py:605
  106.8 0.9 multiply_reduce_fusion
  107.7 0.7 broadcast_in_dim.107.square
  109.4 0.8 multiply_multiply_fusion
  110.2 15.9 %shard_map.201 = bf16[32,2048]{1,0:T(8,128)(2,1)} custom-call(bf16[4,2,32,128]{3,2,1,0:T(8,128)(2,1)} %get-tuple-element.123.conv, f32[4,2,32,128]{3,2,1,0:T(8,128)} %get-tuple-element.122.gated, f32[1,256]{1,0:T(1,128)} %broadcast_in_dim.107.square, f32[1,128]{1,0:T(1,128)} %bitcast.103, bf16[2048,128]{1,0:T(8,128)(2,1)} %get-tuple-element.49.back_conv, ...), custom_call_target="tpu_custom_call" | custom-call | tf_op jit(solution)/shard_map/pallas_call | solution.py:434
  126.2 1.6 %copy.119 = bf16[32,2048]{1,0:T(8,128)(2,1)} copy(bf16[32,2048]{1,0:T(8,128)(2,1)} %shard_map.201) | data formatting | bytes 262144
  (76 shorter events, 6.7 us)
Async XLA Ops:
  0.0 0.7 copy-start
  0.0 1.4 %copy-start.8 = (f32[4,128]{1,0:T(4,128)S(1)}, f32[4,128]{1,0:T(4,128)}, u32[]{:S(2)}) copy-start(f32[4,128]{1,0:T(4,128)} %param.35) | copy-start | bytes 6148
  0.7 0.7 copy-start.12
  0.7 0.7 copy-start.7
  0.7 0.7 copy-start.6
  1.4 0.7 copy-start.4
  2.1 0.8 copy-start.2
  82.4 0.9 copy-start.1
  82.4 0.9 copy-start.9
  103.7 0.7 copy-start.3
  104.3 0.7 copy-start.5
  105.5 1.3 %copy-start.11 = (f32[2,64,128]{2,1,0:T(8,128)S(1)}, f32[2,64,128]{2,1,0:T(8,128)}, u32[]{:S(2)}) copy-start(f32[2,64,128]{2,1,0:T(8,128)} %param.43) | copy-start | bytes 196612
  108.7 0.7 copy-start.10
